TPU v7x, 32 devices: a whole 2x2x4 slice. The times are simulated.
32 devices in a mesh: grp: 2 (over x), ep: 16 (over z, y, core).
Axes of the slice: x: 2, y: 2, z: 4, core: 2. Of those that a mesh axis runs over, the one named last changes fastest.
Arguments:
- tokens: bfloat16 [4096, 2048], P(('grp', 'ep')), parts along dimension 0, may hold values from -6 to 6
- norm_gain: float32 [2048], replicated, may hold values from 0.1 to 1.9
- expert_ids: int32 [4096, 2], P(('grp', 'ep')), parts along dimension 0, may hold values from 0 to 3, all different within a row; in each aligned block of 128 rows (0 to 127, 128 to 255, ...) at most 128 rows name the same one
- route_weight: float32 [4096, 2], P(('grp', 'ep')), parts along dimension 0, may hold values from 0.1 to 1
- gate_weight: bfloat16 [16, 2048, 512], P('ep'), may hold values from -0.375 to 0.375
- up_weight: bfloat16 [16, 2048, 512], P('ep'), may hold values from -0.375 to 0.375
- down_weight: bfloat16 [16, 512, 2048], P('ep'), may hold values from -0.03125 to 0.03125
Outputs:
- combined: bfloat16 [4096, 2048], P(('grp', 'ep')), parts along dimension 0
There are 2 independent parts, one for each index of `grp`. A program takes and returns all parts, laid end to end along the dimension named above; an argument that names none is the same for every part. Nothing has to cross between parts.
Inputs may be any that keep to these rules, and one draw needn't show every extreme that they name: `expert_ids`: each token names 2 different experts; among the tokens of one device no expert is named more than 128 times, and in every draw some expert is named exactly 128 times by the tokens of some device.
All inputs are finite; a program needn't handle non-finite values.
Results may differ from a plain program's by a relative error of at most 0.0078.
Values may be sent and summed in bfloat16 or wider, within the bound.
A program may use at most 128 MiB of HBM per device.

v0:
```python
import jax
import jax.numpy as jnp
from jax import lax
from jax.sharding import PartitionSpec as P

SPLIT = 4


EPSILON = 1e-05
clamp_limit = 7.0
sigmoid_slope = 1.702


def swapped(array, axis, bit):
    return lax.ppermute(array, axis, [(i, i ^ 1 << bit) for i in range(lax.axis_size(axis))])


def layer_norm(tokens, norm_gain):
    values = tokens.astype(jnp.float32)
    center = values - jnp.mean(values, axis=-1, keepdims=True)
    spread = jnp.mean(center * center, axis=-1, keepdims=True)
    return (center * lax.rsqrt(spread + EPSILON) * norm_gain).astype(jnp.bfloat16)


def expert_rows(block_rows, gate_weight, up_weight, down_weight):
    gate_pre = jnp.einsum(
        "scd,df->scf", block_rows, gate_weight[0], preferred_element_type=jnp.float32
    )
    up_pre = jnp.einsum("scd,df->scf", block_rows, up_weight[0], preferred_element_type=jnp.float32)
    gate_cut = jnp.minimum(gate_pre, clamp_limit)
    up_cut = jnp.clip(up_pre, -clamp_limit, clamp_limit)
    active = ((up_cut + 1.0) * (gate_cut * jax.nn.sigmoid(gate_cut * sigmoid_slope))).astype(
        jnp.bfloat16
    )
    return jnp.einsum("scf,fd->scd", active, down_weight[0], preferred_element_type=jnp.float32)


def body(tokens, norm_gain, expert_ids, route_weight, gate_weight, up_weight, down_weight):
    normed = layer_norm(tokens, norm_gain)
    devices = lax.axis_size("ep")
    experts = devices // SPLIT
    tok_rows = tokens.shape[0]
    top_count = expert_ids.shape[1]
    width = tokens.shape[1]
    capacity = min(tok_rows, 2 * tok_rows * top_count // experts)
    quarter = capacity // SPLIT
    levels = SPLIT.bit_length() - 1
    position = lax.axis_index("ep")
    flat_ids = expert_ids.reshape(-1)
    onehot = (flat_ids[:, None] == jnp.arange(experts, dtype=jnp.int32)[None, :]).astype(jnp.int32)
    earlier = jnp.cumsum(onehot, axis=0) - onehot
    slot_index = jnp.sum(earlier * onehot, axis=1)
    target = flat_ids * capacity + slot_index
    owners = jnp.arange(flat_ids.shape[0], dtype=jnp.int32) // top_count
    slot_token = jnp.full((experts * capacity,), tok_rows, jnp.int32).at[target].set(owners)
    padded = jnp.concatenate([normed, jnp.zeros((1, width), jnp.bfloat16)], axis=0)
    outgoing = jnp.take(padded, slot_token, axis=0).reshape(experts, capacity, width)
    pieces = outgoing.reshape(devices, quarter, width)
    gathered = lax.all_to_all(pieces, "ep", split_axis=0, concat_axis=0, tiled=True)
    for bit_level in range(levels):
        partner = swapped(gathered, "ep", bit_level)
        upper_bit = position >> bit_level & 1
        first_half = jnp.where(upper_bit == 1, partner, gathered)
        second_half = jnp.where(upper_bit == 1, gathered, partner)
        gathered = jnp.concatenate([first_half, second_half], axis=1)
    partial_value = expert_rows(gathered, gate_weight, up_weight, down_weight)
    length = capacity
    for bit_level in reversed(range(levels)):
        length = length // 2
        upper_bit = position >> bit_level & 1
        kept_rows = lax.dynamic_slice_in_dim(partial_value, upper_bit * length, length, 1)
        sent_rows = lax.dynamic_slice_in_dim(partial_value, (1 - upper_bit) * length, length, 1)
        partial_value = kept_rows + swapped(sent_rows, "ep", bit_level)
    finished = partial_value.astype(jnp.bfloat16)
    returned = lax.all_to_all(finished, "ep", split_axis=0, concat_axis=0, tiled=True)
    results = returned.reshape(experts * capacity, width)
    picked = jnp.take(results, target, axis=0).reshape(tok_rows, top_count, width)
    combined = jnp.sum(route_weight[:, :, None] * picked.astype(jnp.float32), axis=1)
    return combined.astype(jnp.bfloat16)


def solution(mesh):
    placed = (
        P(("grp", "ep"), None),
        P(),
        P(("grp", "ep"), None),
        P(("grp", "ep"), None),
        P("ep", None, None),
        P("ep", None, None),
        P("ep", None, None),
    )
    return jax.shard_map(
        body, mesh=mesh, in_specs=placed, out_specs=P(("grp", "ep"), None), check_vma=False
    )
```

profile of v0, /device:TPU:0, one launch (start us, length us, event | category | flops | bytes accessed | tf_op | source)
XLA Modules:
  0.0 480.6 jit_solution(8666574358104673671)
XLA Ops:
  3.8 1.4 scatter_custom_fusion
  7.9 1.4 fusion.15
  9.4 3.3 gather_fusion
  12.7 1.8 broadcast_select_fusion.2
  14.6 54.5 %all_to_all.10 = bf16[16,32,2048]{2,1,0:T(8,128)(2,1)} all-to-all(bf16[16,32,2048]{2,1,0:T(8,128)(2,1)S(1)} %broadcast_select_fusion.2), channel_id=1, replica_groups=mesh['grp'=2,'ep'=16] {'ep'}, dimensions={0} | all-to-all | bytes 4194304 | tf_op jit(solution)/shard_map/all_to_all | solution.py:59
  70.0 4.1 collective-permute-done
  74.1 2.5 broadcast_select_fusion.4
  76.6 2.9 pad_maximum_fusion.3
  81.2 91.9 %collective-permute-done.1 = bf16[16,64,2048]{2,1,0:T(8,128)(2,1)} collective-permute-done((bf16[16,64,2048]{2,1,0:T(8,128)(2,1)}, bf16[16,64,2048]{2,1,0:T(8,128)(2,1)}, u32[]{:S(2)}, u32[]{:S(2)}) %collective-permute-start.1) | collective-permute-done | bytes 4194336 | tf_op jit(solution)/shard_map/ppermute | solution.py:15
  173.1 4.5 broadcast_select_fusion.1
  177.6 2.0 copy-done.4
  180.9 6.1 %fusion.1 = f32[16,128,512]{2,1,0:T(8,128)} fusion(bf16[16,64,2048]{2,1,0:T(8,128)(2,1)S(1)} %get-tuple-element.6, bf16[16,64,2048]{2,1,0:T(8,128)(2,1)S(1)} %get-tuple-element.5, bf16[1,2048,512]{2,1,0:T(8,128)(2,1)S(1)} %copy-done.8), kind=kOutput, calls=%fused_computation.6 | convolution fusion | flops 4311744512 | bytes 14680064 | tf_op jit(solution)/shard_map/scd,df->scf/dot_general | solution.py:29
  186.9 16.5 %fusion.2 = f32[16,128,2048]{2,1,0:T(8,128)} fusion(f32[16,128,512]{2,1,0:T(8,128)} %fusion.1, bf16[16,64,2048]{2,1,0:T(8,128)(2,1)} %copy-done.5, bf16[16,64,2048]{2,1,0:T(8,128)(2,1)} %copy-done.4, bf16[1,512,2048]{2,1,0:T(8,128)(2,1)S(1)} %copy-done, bf16[1,2048,512]{2,1,0:T(8,128)(2,1)} %param.11), kind=kOutput, calls=%fused_computation.12 | convolution fusion | flops 8617197568 | bytes 33554432 | tf_op jit(solution)/shard_map/scf,fd->scd/dot_general | solution.py:35
  203.4 7.7 %constant_dynamic-slice_fusion = f32[16,64,2048]{2,1,0:T(8,128)} fusion(f32[16,128,2048]{2,1,0:T(8,128)} %fusion.2, s32[]{:T(128)S(6)} %select_n.85), kind=kLoop, calls=%fused_computation.52 | loop fusion | bytes 16777220 | tf_op jit(solution)/shard_map/dynamic_slice | solution.py:72
  212.4 181.0 %collective-permute-done.2 = f32[16,64,2048]{2,1,0:T(8,128)} collective-permute-done((f32[16,64,2048]{2,1,0:T(8,128)}, f32[16,64,2048]{2,1,0:T(8,128)}, u32[]{:S(2)}, u32[]{:S(2)}) %collective-permute-start.2) | collective-permute-done | bytes 8388640 | tf_op jit(solution)/shard_map/ppermute | solution.py:15
  393.4 11.7 %dynamic-slice_add_fusion = f32[16,64,2048]{2,1,0:T(8,128)} fusion(f32[16,64,2048]{2,1,0:T(8,128)} %collective-permute-done.2, f32[16,128,2048]{2,1,0:T(8,128)} %fusion.2, s32[]{:T(128)S(6)} %select_n.84), kind=kLoop, calls=%fused_computation.4 | loop fusion | flops 2097152 | bytes 25165828 | tf_op jit(solution)/shard_map/add | solution.py:73
  405.1 4.7 constant_dynamic-slice_fusion.1
  409.7 7.5 %collective-permute-done.3 = f32[16,32,2048]{2,1,0:T(8,128)} collective-permute-done((f32[16,32,2048]{2,1,0:T(8,128)}, f32[16,32,2048]{2,1,0:T(8,128)}, u32[]{:S(2)}, u32[]{:S(2)}) %collective-permute-start.3) | collective-permute-done | bytes 4194336 | tf_op jit(solution)/shard_map/ppermute | solution.py:15
  417.2 5.4 %add_convert_fusion = bf16[16,32,2048]{2,1,0:T(8,128)(2,1)} fusion(f32[16,32,2048]{2,1,0:T(8,128)} %collective-permute-done.3, f32[16,64,2048]{2,1,0:T(8,128)} %dynamic-slice_add_fusion, s32[]{:T(128)S(6)} %select_n.86), kind=kLoop, calls=%fused_computation.8 | loop fusion | flops 2097152 | bytes 10485764 | tf_op jit(solution)/shard_map/convert_element_type | solution.py:74
  422.7 4.8 %all-to-all-start.1 = ((bf16[16,32,2048]{2,1,0:T(8,128)(2,1)}), bf16[16,32,2048]{2,1,0:T(8,128)(2,1)}, u32[]{:S(2)}, u32[]{:S(2)}) async-start(bf16[16,32,2048]{2,1,0:T(8,128)(2,1)} %add_convert_fusion), calls=%async_computation.1 | async-start | bytes 4194304 | tf_op jit(solution)/shard_map/all_to_all | solution.py:75
  428.0 40.4 %all-to-all-done.1 = bf16[16,32,2048]{2,1,0:T(8,128)(2,1)} async-done(((bf16[16,32,2048]{2,1,0:T(8,128)(2,1)}), bf16[16,32,2048]{2,1,0:T(8,128)(2,1)}, u32[]{:S(2)}, u32[]{:S(2)}) %all-to-all-start.1) | async-done | bytes 2097184 | tf_op jit(solution)/shard_map/all_to_all | solution.py:75
  468.4 4.4 gather_fusion.1
  472.8 1.5 gather.15
  474.3 6.2 %multiply_reduce_fusion = bf16[128,2048]{1,0:T(8,128)(2,1)} fusion(bf16[128,2,2048]{2,1,0:T(2,128)(2,1)} %gather.15, pred[128,2]{1,0:T(8,128)(4,1)S(1)} %copy.24, f32[128,2]{1,0:T(8,128)S(1)} %copy.18), kind=kLoop, calls=%fused_computation.16 | loop fusion | flops 1835008 | bytes 1574144 | tf_op jit(solution)/shard_map/reduce_sum | solution.py:78
  (53 shorter events, 12.1 us)
Async XLA Ops:
  0.0 186.9 %copy-start = (bf16[1,512,2048]{2,1,0:T(8,128)(2,1)S(1)}, bf16[1,512,2048]{2,1,0:T(8,128)(2,1)}, u32[]{:S(2)}) copy-start(bf16[1,512,2048]{2,1,0:T(8,128)(2,1)} %param.13) | copy-start | bytes 6291460
  69.0 5.1 %collective-permute-start = (bf16[16,32,2048]{2,1,0:T(8,128)(2,1)}, bf16[16,32,2048]{2,1,0:T(8,128)(2,1)}, u32[]{:S(2)}, u32[]{:S(2)}) collective-permute-start(bf16[16,32,2048]{2,1,0:T(8,128)(2,1)} %all_to_all.10), channel_id=1, source_target_pairs={{0,1},{1,0},{2,3},{3,2},{4,5},{5,4},{6,7},{7,6},{8,9},{9,8},{10,11... | collective-permute-start | bytes 6291464 | tf_op jit(solution)/shard_map/ppermute | solution.py:15
  76.6 3.0 copy-start.2
  76.6 3.3 copy-start.3
  79.9 93.2 %collective-permute-start.1 = (bf16[16,64,2048]{2,1,0:T(8,128)(2,1)}, bf16[16,64,2048]{2,1,0:T(8,128)(2,1)}, u32[]{:S(2)}, u32[]{:S(2)}) collective-permute-start(bf16[16,64,2048]{2,1,0:T(8,128)(2,1)} %pad_maximum_fusion.3), channel_id=1, source_target_pairs={{0,2},{1,3},{2,0},{3,1},{4,6},{5,7},{6,4},{7,5},{8,10},{9,11},{10,... | collective-permute-start | bytes 12582920 | tf_op jit(solution)/shard_map/ppermute | solution.py:15
  81.2 99.7 %copy-start.8 = (bf16[1,2048,512]{2,1,0:T(8,128)(2,1)S(1)}, bf16[1,2048,512]{2,1,0:T(8,128)(2,1)}, u32[]{:S(2)}) copy-start(bf16[1,2048,512]{2,1,0:T(8,128)(2,1)} %param.12) | copy-start | bytes 6291460
  177.6 2.0 copy-start.4
  177.6 3.2 copy-start.5
  211.1 182.2 %collective-permute-start.2 = (f32[16,64,2048]{2,1,0:T(8,128)}, f32[16,64,2048]{2,1,0:T(8,128)}, u32[]{:S(2)}, u32[]{:S(2)}) collective-permute-start(f32[16,64,2048]{2,1,0:T(8,128)} %constant_dynamic-slice_fusion), channel_id=1, source_target_pairs={{0,2},{1,3},{2,0},{3,1},{4,6},{5,7},{6,4},{7,5},{8,10},{9,11},{10,... | collective-permute-start | bytes 25165832 | tf_op jit(solution)/shard_map/ppermute | solution.py:15
  409.7 7.5 %collective-permute-start.3 = (f32[16,32,2048]{2,1,0:T(8,128)}, f32[16,32,2048]{2,1,0:T(8,128)}, u32[]{:S(2)}, u32[]{:S(2)}) collective-permute-start(f32[16,32,2048]{2,1,0:T(8,128)} %constant_dynamic-slice_fusion.1), channel_id=1, source_target_pairs={{0,1},{1,0},{2,3},{3,2},{4,5},{5,4},{6,7},{7,6},{8,9},{9,8},{10,11... | collective-permute-start | bytes 12582920 | tf_op jit(solution)/shard_map/ppermute | solution.py:15
  422.7 5.0 %copy-start.6 = (s32[128,2]{0,1:T(2,128)S(1)}, s32[128,2]{0,1:T(2,128)}, u32[]{:S(2)}) copy-start(s32[128,2]{0,1:T(2,128)} %param.9) | copy-start | bytes 3076
  422.7 5.2 %copy-start.7 = (f32[128,2]{0,1:T(2,128)S(1)}, f32[128,2]{0,1:T(2,128)}, u32[]{:S(2)}) copy-start(f32[128,2]{0,1:T(2,128)} %param.10) | copy-start | bytes 3076
  422.7 45.8 %all-to-all-start.1 = ((bf16[16,32,2048]{2,1,0:T(8,128)(2,1)}), bf16[16,32,2048]{2,1,0:T(8,128)(2,1)}, u32[]{:S(2)}, u32[]{:S(2)}) async-start(bf16[16,32,2048]{2,1,0:T(8,128)(2,1)} %add_convert_fusion), calls=%async_computation.1 | async-start | bytes 4194304 | tf_op jit(solution)/shard_map/all_to_all | solution.py:75
  468.4 12.1 %copy-start.1 = (bf16[1,512,2048]{2,1,0:T(8,128)(2,1)S(1)}, bf16[1,512,2048]{2,1,0:T(8,128)(2,1)}, u32[]{:S(2)}) copy-start(bf16[1,512,2048]{2,1,0:T(8,128)(2,1)} %param.13) | copy-start | bytes 6291460
where the time goes:
time: 487 us; the launch traced here: 481 us
  waiting for transfers between devices  325 us (67%)
  blocking collectives  54.5 us (11%)
  other arithmetic  41.2 us (8%)
  local copies, waits for them, and re-layouts  28.9 us (6%)
  matrix products  22.6 us (5%)
  starting transfers between devices  8.32 us (2%)
    ppermute x4, waiting for transfers between devices, swapped(): lax.ppermute(array, axis, [(i, i ^ 1 << bit) for i in range(lax.axis_size...  285 us
    all_to_all x1, blocking collectives, body(): lax.all_to_all(pieces, 'ep', split_axis=0, concat_axis=0, tiled=True)  54.5 us
    all_to_all x1, waiting for transfers between devices, body(): lax.all_to_all(finished, 'ep', split_axis=0, concat_axis=0, tiled=True)  40.4 us
    dot_general x1, matrix products, expert_rows(): jnp.einsum('scf,fd->scd', active, down_weight[0], preferred_element_type=...  16.5 us
    dynamic_slice x2, local copies, waits for them, and re-layouts, body(): lax.dynamic_slice_in_dim(partial_value, (1 - upper_bit) * length, length, 1)  12.4 us
    add x1, other arithmetic, body(): partial_value = kept_rows + swapped(sent_rows, 'ep', bit_level)  11.7 us
  transfers between devices with their start and end apart: 5, of which 5 were waited for; matrix products, arithmetic and copies ran while one was open for 0% of the time, Pallas kernels for 0%

commit v1 on v0

--- a/solution.py
+++ b/solution.py
@@ -1,6 +1,10 @@
+import functools
+
 import jax
 import jax.numpy as jnp
 from jax import lax
+from jax.experimental import pallas as pl
+from jax.experimental.pallas import tpu as pltpu
 from jax.sharding import PartitionSpec as P
 
 SPLIT = 4
@@ -35,7 +39,7 @@
     return jnp.einsum("scf,fd->scd", active, down_weight[0], preferred_element_type=jnp.float32)
 
 
-def body(tokens, norm_gain, expert_ids, route_weight, gate_weight, up_weight, down_weight):
+def slot_body(tokens, norm_gain, expert_ids, route_weight, gate_weight, up_weight, down_weight):
     normed = layer_norm(tokens, norm_gain)
     devices = lax.axis_size("ep")
     experts = devices // SPLIT
@@ -79,6 +83,346 @@
     return combined.astype(jnp.bfloat16)
 
 
+MESH = pl.DeviceIdType.MESH
+HALVES = 2
+
+
+def near_plane(z, k, planes):
+    below, above = z, planes - 1 - z
+    short = jnp.minimum(below, above)
+    side = jnp.where(above >= below, 1, -1)
+    paired = jnp.where(k % 2 == 1, side * ((k + 1) // 2), -side * (k // 2))
+    return z + jnp.where(k <= 2 * short, paired, side * (k - short))
+
+
+def lane_to_column(row, rows):
+    eye = lax.broadcasted_iota(jnp.int32, (rows, rows), 0) == lax.broadcasted_iota(
+        jnp.int32, (rows, rows), 1
+    )
+    return jnp.sum(jnp.where(eye, row, 0.0), axis=1, keepdims=True)
+
+
+def column_to_lane(column, rows):
+    eye = lax.broadcasted_iota(jnp.int32, (rows, rows), 0) == lax.broadcasted_iota(
+        jnp.int32, (rows, rows), 1
+    )
+    return jnp.sum(jnp.where(eye, column, 0.0), axis=0, keepdims=True)
+
+
+def dense_kernel(
+    devices,
+    tokens_ref, gain_ref, ids_ref, route_ref, gate_hbm, up_hbm, down_hbm,
+    out_ref,
+    tok, part, cbuf, ybuf, zbuf, acc, wsend, wbuf, gate, up, down,
+    wsem, gsend, grecv, rsend_c, rrecv_c, rsend_y, rrecv_y, rsend_z, rrecv_z, ssend, srecv,
+):
+    planes = devices // SPLIT
+    rows, width = tokens_ref.shape
+    half = rows // HALVES
+    me = lax.axis_index("ep")
+    z, y, c = me // 4, (me // 2) % 2, me % 2
+
+    def index(zp, yp, cp):
+        return zp * 4 + yp * 2 + cp
+
+    ypeer, cpeer = index(z, 1 - y, c), index(z, y, 1 - c)
+
+    def span(h):
+        return pl.ds(h * half, half)
+
+    def remote(source, target, send_sem, recv_sem, device):
+        return pltpu.make_async_remote_copy(
+            src_ref=source, dst_ref=target, send_sem=send_sem, recv_sem=recv_sem,
+            device_id={"ep": device}, device_id_type=MESH,
+        )
+
+    def move(kind, i, h, device):
+        return remote(
+            tok.at[i, span(h)], tok.at[i, span(h)], gsend.at[kind, i, h], grecv.at[i, h], device
+        )
+
+    weight_loads = [
+        pltpu.make_async_copy(gate_hbm.at[0], gate, wsem.at[0]),
+        pltpu.make_async_copy(up_hbm.at[0], up, wsem.at[1]),
+        pltpu.make_async_copy(down_hbm.at[0], down, wsem.at[2]),
+    ]
+    for load in weight_loads:
+        load.start()
+
+    barrier = pltpu.get_barrier_semaphore()
+    for step in range(1, devices):
+        pl.semaphore_signal(
+            barrier, inc=1, device_id={"ep": (me + step) % devices}, device_id_type=MESH
+        )
+    for h in range(HALVES):
+        values = tokens_ref[span(h), :].astype(jnp.float32)
+        center = values - jnp.mean(values, axis=-1, keepdims=True)
+        spread = jnp.mean(center * center, axis=-1, keepdims=True)
+        tok[me, span(h), :] = (center * lax.rsqrt(spread + EPSILON) * gain_ref[...]).astype(
+            jnp.bfloat16
+        )
+    for e in range(planes):
+        column = jnp.sum(jnp.where(ids_ref[...] == e, route_ref[...], 0.0), axis=1, keepdims=True)
+        wsend[e] = jnp.broadcast_to(column_to_lane(column, rows), (8, rows))
+    pl.semaphore_wait(barrier, devices - 1)
+
+    has_up, has_down = z < planes - 1, z > 0
+    for h in range(HALVES):
+        move(2, me, h, ypeer).start()
+        pl.when(has_up)(lambda: move(0, me, h, me + 4).start())
+        pl.when(has_down)(lambda: move(1, me, h, me - 4).start())
+        move(3, me, h, cpeer).start()
+
+    def share(step):
+        there = (me + step) % devices
+        return remote(wsend.at[there // SPLIT], wbuf.at[me], ssend.at[there], srecv.at[me], there)
+
+    def shared(step):
+        there = (me + step) % devices
+        return remote(wsend.at[z], wbuf.at[there], ssend.at[there], srecv.at[there], there)
+
+    for step in range(1, devices):
+        share(step).start()
+    wbuf[me] = wsend[z]
+    for load in weight_loads:
+        load.wait()
+    for step in range(1, devices):
+        shared(step).wait_recv()
+
+    def onward(zp):
+        return jnp.where(zp < z, z + 1, z - 1)
+
+    def exists(plane):
+        return jnp.logical_and(plane >= 0, plane < planes)
+
+    def compute(zp, yp):
+        first = index(zp, yp, 0)
+        x = tok[pl.ds(first, 2)].reshape(2 * rows, width)
+        gate_cut = jnp.minimum(
+            jnp.dot(x, gate[...], preferred_element_type=jnp.float32), clamp_limit
+        )
+        up_cut = jnp.clip(
+            jnp.dot(x, up[...], preferred_element_type=jnp.float32), -clamp_limit, clamp_limit
+        )
+        active = ((up_cut + 1.0) * (gate_cut * jax.nn.sigmoid(gate_cut * sigmoid_slope))).astype(
+            jnp.bfloat16
+        )
+        scale = jnp.concatenate(
+            [lane_to_column(wbuf[first + lane, 0:1, :], rows) for lane in range(2)], axis=0
+        )
+        tile = min(512, width)
+        for start in range(0, width, tile):
+            value = jnp.dot(
+                active, down[:, start : start + tile], preferred_element_type=jnp.float32
+            )
+            part[pl.ds(first, 2), :, start : start + tile] = (
+                (value * scale).astype(jnp.bfloat16).reshape(2, rows, tile)
+            )
+
+    def to_core(zp, yp):
+        group = zp * 2 + yp
+        return remote(
+            part.at[index(zp, yp, 1 - c)], cbuf.at[group],
+            rsend_c.at[group], rrecv_c.at[group], cpeer,
+        )
+
+    def gather_step(k, _):
+        zk = near_plane(z, jnp.minimum(k, planes - 1), planes)
+        zb = near_plane(z, jnp.maximum(k - 1, 0), planes)
+
+        @pl.when(jnp.logical_and(k > 0, k < planes))
+        def _():
+            i = index(zk, y, c)
+            nz = onward(zk)
+            for h in range(HALVES):
+                move(2, i, h, ypeer).wait_recv()
+                pl.when(exists(nz))(lambda: move(0, i, h, index(nz, y, c)).start())
+                move(2, i, h, ypeer).start()
+                move(3, i, h, cpeer).start()
+
+        @pl.when(k > 0)
+        def _():
+            i = index(zb, 1 - y, c)
+            for h in range(HALVES):
+                move(3, i, h, cpeer).wait_recv()
+                move(3, i, h, cpeer).start()
+
+        def group_step(j, _):
+            zp = jnp.where(j == 0, zk, zb)
+            yp = jnp.where(j == 0, y, 1 - y)
+
+            @pl.when(jnp.where(j == 0, planes - k, k) > 0)
+            def _():
+                for h in range(HALVES):
+                    move(3, index(zp, yp, 1 - c), h, cpeer).wait_recv()
+                compute(zp, yp)
+                to_core(zp, yp).start()
+
+            return 0
+
+        lax.fori_loop(0, 2, group_step, 0)
+        return 0
+
+    lax.fori_loop(0, planes + 1, gather_step, 0)
+
+    def to_y(zp, h):
+        return remote(
+            part.at[index(zp, 1 - y, c), span(h)], ybuf.at[zp, span(h)],
+            rsend_y.at[zp, h], rrecv_y.at[zp, h], ypeer,
+        )
+
+    def from_y(zp, h):
+        return remote(
+            part.at[index(zp, y, c), span(h)], ybuf.at[zp, span(h)],
+            rsend_y.at[zp, h], rrecv_y.at[zp, h], ypeer,
+        )
+
+    def spread_step(t, _):
+        zp = near_plane(z, planes - 1 - t, planes)
+        to_core(zp, 1 - y).wait_recv()
+        i = index(zp, 1 - y, c)
+        for h in range(HALVES):
+            part[i, span(h), :] = (
+                part[i, span(h), :].astype(jnp.float32)
+                + cbuf[zp * 2 + 1 - y, span(h), :].astype(jnp.float32)
+            ).astype(jnp.bfloat16)
+            to_y(zp, h).start()
+        return 0
+
+    lax.fori_loop(0, planes, spread_step, 0)
+
+    def hop(zp, h):
+        nz = jnp.where(zp > z, z + 1, z - 1)
+        slot = jnp.where(jnp.logical_and(nz == zp, zp < z), planes, zp)
+        return remote(
+            part.at[index(zp, y, c), span(h)], zbuf.at[slot, span(h)],
+            rsend_z.at[zp, h], rrecv_z.at[slot, h], index(nz, y, c),
+        )
+
+    def landed(slot, h):
+        return remote(
+            part.at[me, span(h)], zbuf.at[slot, span(h)],
+            rsend_z.at[z, h], rrecv_z.at[slot, h], ypeer,
+        )
+
+    def add_landed(slot, h):
+        landed(slot, h).wait_recv()
+        acc[...] += zbuf[slot, span(h), :].astype(jnp.float32)
+
+    def total(zp, h):
+        from_y(zp, h).wait_recv()
+        acc[...] = (
+            part[index(zp, y, c), span(h), :].astype(jnp.float32)
+            + cbuf[zp * 2 + y, span(h), :].astype(jnp.float32)
+            + ybuf[zp, span(h), :].astype(jnp.float32)
+        )
+
+    def chain_step(t, _):
+        zp = near_plane(z, planes - 1 - t, planes)
+        to_core(zp, y).wait_recv()
+        for h in range(HALVES):
+            total(zp, h)
+            pl.when(jnp.where(zp > z, has_down, has_up))(lambda: add_landed(zp, h))
+            part[index(zp, y, c), span(h), :] = acc[...].astype(jnp.bfloat16)
+            hop(zp, h).start()
+        return 0
+
+    lax.fori_loop(0, planes - 1, chain_step, 0)
+    to_core(z, y).wait_recv()
+    for h in range(HALVES):
+        total(z, h)
+        pl.when(has_down)(lambda: add_landed(z, h))
+        pl.when(has_up)(lambda: add_landed(planes, h))
+        out_ref[span(h), :] = acc[...].astype(jnp.bfloat16)
+
+    for step in range(1, devices):
+        share(step).wait_send()
+    for h in range(HALVES):
+        move(2, me, h, ypeer).wait_send()
+        pl.when(has_up)(lambda: move(0, me, h, me + 4).wait_send())
+        pl.when(has_down)(lambda: move(1, me, h, me - 4).wait_send())
+        move(3, me, h, cpeer).wait_send()
+
+    def drain_step(k, _):
+        zp = near_plane(z, k, planes)
+        to_core(zp, y).wait_send()
+        to_core(zp, 1 - y).wait_send()
+        for h in range(HALVES):
+            move(3, index(zp, 1 - y, c), h, cpeer).wait_send()
+            to_y(zp, h).wait_send()
+
+        @pl.when(k > 0)
+        def _():
+            i = index(zp, y, c)
+            nz = onward(zp)
+            for h in range(HALVES):
+                pl.when(exists(nz))(lambda: move(0, i, h, index(nz, y, c)).wait_send())
+                move(2, i, h, ypeer).wait_send()
+                move(3, i, h, cpeer).wait_send()
+                hop(zp, h).wait_send()
+
+        return 0
+
+    lax.fori_loop(0, planes, drain_step, 0)
+
+
+def dense_body(tokens, norm_gain, expert_ids, route_weight, gate_weight, up_weight, down_weight):
+    devices = lax.axis_size("ep")
+    planes = devices // SPLIT
+    rows, width = tokens.shape
+    hidden = gate_weight.shape[2]
+    half = rows // HALVES
+    vmem, dma = pltpu.VMEM, pltpu.SemaphoreType.DMA
+    block = jnp.bfloat16
+    return pl.pallas_call(
+        functools.partial(dense_kernel, devices),
+        out_shape=jax.ShapeDtypeStruct((rows, width), block),
+        in_specs=[pl.BlockSpec(memory_space=vmem)] * 4 + [pl.BlockSpec(memory_space=pl.ANY)] * 3,
+        out_specs=pl.BlockSpec(memory_space=vmem),
+        scratch_shapes=[
+            vmem((devices, rows, width), block),
+            vmem((devices, rows, width), block),
+            vmem((2 * planes, rows, width), block),
+            vmem((planes, rows, width), block),
+            vmem((planes + 1, rows, width), block),
+            vmem((half, width), jnp.float32),
+            vmem((planes, 8, rows), jnp.float32),
+            vmem((devices, 8, rows), jnp.float32),
+            vmem((width, hidden), block),
+            vmem((width, hidden), block),
+            vmem((hidden, width), block),
+            dma((3,)),
+            dma((4, devices, HALVES)),
+            dma((devices, HALVES)),
+            dma((2 * planes,)),
+            dma((2 * planes,)),
+            dma((planes, HALVES)),
+            dma((planes, HALVES)),
+            dma((planes, HALVES)),
+            dma((planes + 1, HALVES)),
+            dma((devices,)),
+            dma((devices,)),
+        ],
+        compiler_params=pltpu.CompilerParams(
+            collective_id=0, has_side_effects=True, vmem_limit_bytes=60 * 1024 * 1024
+        ),
+        name="dense_experts",
+    )(
+        tokens, norm_gain.reshape(1, width), expert_ids, route_weight,
+        gate_weight, up_weight, down_weight,
+    )
+
+
+def body(tokens, norm_gain, expert_ids, route_weight, gate_weight, up_weight, down_weight):
+    tok_rows, top_count = expert_ids.shape
+    experts = lax.axis_size("ep") // SPLIT
+    capacity = min(tok_rows, 2 * tok_rows * top_count // experts)
+    chosen = dense_body if capacity == tok_rows else slot_body
+    return chosen(
+        tokens, norm_gain, expert_ids, route_weight, gate_weight, up_weight, down_weight
+    )
+
+
 def solution(mesh):
     placed = (
         P(("grp", "ep"), None),

time: 487 us -> 120 us (0.25); the launches traced: 481 us -> 119 us
  waiting for transfers between devices: 325 us -> 0 us
  Pallas kernels: 0 us -> 115 us
  blocking collectives: 54.5 us -> 0 us
  other arithmetic: 41.2 us -> 0 us
  local copies, waits for them, and re-layouts: 28.9 us -> 4.7 us
  matrix products: 22.6 us -> 0 us
  starting transfers between devices: 8.32 us -> 0 us
    ppermute x4 -> x0, waiting for transfers between devices: 285 us -> none  [swapped(): lax.ppermute(array, axis, [(i, i ^ 1 << bit) for i in range(lax.axis_size...]
    pallas_call x0 -> x1, Pallas kernels: none -> 115 us  [dense_body(): pl.pallas_call(functools.partial(dense_kernel, devices), out_shape=jax.Sh...]
    all_to_all x1 -> x0, blocking collectives: 54.5 us -> none  [body(): lax.all_to_all(pieces, 'ep', split_axis=0, concat_axis=0, tiled=True)]
    all_to_all x1 -> x0, waiting for transfers between devices: 40.4 us -> none  [body(): lax.all_to_all(finished, 'ep', split_axis=0, concat_axis=0, tiled=True)]
    dot_general x2 -> x0, matrix products: 22.6 us -> none  [the longest x1 16.5 us: expert_rows(): jnp.einsum('scf,fd->scd', active, down_weight[0], preferred_element_type=...]
    dynamic_slice x2 -> x0, local copies, waits for them, and re-layouts: 12.4 us -> none  [body(): lax.dynamic_slice_in_dim(partial_value, (1 - upper_bit) * length, length, 1)]
    add x1 -> x0, other arithmetic: 11.7 us -> none  [body(): partial_value = kept_rows + swapped(sent_rows, 'ep', bit_level)]
    gather x3 -> x0, local copies, waits for them, and re-layouts: 9.24 us -> none  [the longest x2 5.89 us: body(): jnp.take(results, target, axis=0).reshape(tok_rows, top_count, width)]
  transfers between devices with their start and end apart: 5 -> 0, of which waited for: 5 -> 0; matrix products, arithmetic and copies ran while one was open for 0% -> 0% of each run, Pallas kernels for 0% -> 0%
where the time goes in v1:
time: 120 us; the launch traced here: 119 us
  Pallas kernels  115 us (96%)
  local copies, waits for them, and re-layouts  4.7 us (4%)
    pallas_call x1, Pallas kernels, dense_body(): pl.pallas_call(functools.partial(dense_kernel, devices), out_shape=jax.Sh...  115 us
    unnamed x3, local copies, waits for them, and re-layouts  4.7 us

profile of v1, /device:TPU:0, one launch (start us, length us, event | category | flops | bytes accessed | tf_op | source)
XLA Modules:
  0.0 119.5 jit_solution(10601550747447420271)
XLA Ops:
  0.0 1.4 %copy.8.ids_ref = s32[128,2]{1,0:T(8,128)} copy(s32[128,2]{0,1:T(2,128)} %param.9) | data formatting | bytes 2048 | tf_op args[2]
  1.4 1.4 %copy.9.route_ref = f32[128,2]{1,0:T(8,128)} copy(f32[128,2]{0,1:T(2,128)} %param.10) | data formatting | bytes 2048 | tf_op args[3]
  2.8 114.8 %dense_experts.1 = bf16[128,2048]{1,0:T(8,128)(2,1)} custom-call(bf16[128,2048]{1,0:T(8,128)(2,1)} %tokens_ref.1, f32[1,2048]{1,0:T(1,128)} %bitcast.1, s32[128,2]{1,0:T(8,128)} %copy.8.ids_ref, f32[128,2]{1,0:T(8,128)} %copy.9.route_ref, bf16[1,2048,512]{2,1,0:T(8,128)(2,1)} %gate_hbm.1, bf16[1,2048,512]{2,1,0:T(8,128)(2,1)} %up_hbm.1, ...), custom_call_target="tpu_custom_call" | custom-call | tf_op jit(solution)/shard_map/dense_experts/pallas_call | solution.py:377
  117.6 1.9 %copy.11 = bf16[128,2048]{1,0:T(8,128)(2,1)} copy(bf16[128,2048]{1,0:T(8,128)(2,1)} %dense_experts.1) | data formatting | bytes 1048576

commit v2 on v1

--- a/solution.py
+++ b/solution.py
@@ -85,6 +85,7 @@
 
 MESH = pl.DeviceIdType.MESH
 HALVES = 2
+LANES = 128
 
 
 def near_plane(z, k, planes):
@@ -102,19 +103,12 @@
     return jnp.sum(jnp.where(eye, row, 0.0), axis=1, keepdims=True)
 
 
-def column_to_lane(column, rows):
-    eye = lax.broadcasted_iota(jnp.int32, (rows, rows), 0) == lax.broadcasted_iota(
-        jnp.int32, (rows, rows), 1
-    )
-    return jnp.sum(jnp.where(eye, column, 0.0), axis=0, keepdims=True)
-
-
 def dense_kernel(
     devices,
     tokens_ref, gain_ref, ids_ref, route_ref, gate_hbm, up_hbm, down_hbm,
     out_ref,
-    tok, part, cbuf, ybuf, zbuf, acc, wsend, wbuf, gate, up, down,
-    wsem, gsend, grecv, rsend_c, rrecv_c, rsend_y, rrecv_y, rsend_z, rrecv_z, ssend, srecv,
+    tok, part, cbuf, ybuf, zbuf, acc, gate, up, down,
+    wsem, gsend, grecv, rsend_c, rrecv_c, rsend_y, rrecv_y, rsend_z, rrecv_z,
 ):
     planes = devices // SPLIT
     rows, width = tokens_ref.shape
@@ -149,45 +143,45 @@
     for load in weight_loads:
         load.start()
 
+    has_up, has_down = z < planes - 1, z > 0
     barrier = pltpu.get_barrier_semaphore()
-    for step in range(1, devices):
+
+    def greet(device):
         pl.semaphore_signal(
-            barrier, inc=1, device_id={"ep": (me + step) % devices}, device_id_type=MESH
-        )
+            barrier, inc=1, device_id={"ep": device}, device_id_type=MESH
+        )
+
+    greet(ypeer)
+    greet(cpeer)
+    pl.when(has_up)(lambda: greet(me + 4))
+    pl.when(has_down)(lambda: greet(me - 4))
+
+    lanes = lax.broadcasted_iota(jnp.int32, (1, LANES), 1)
+    routes = jnp.zeros((rows, LANES), jnp.float32)
+    for e in range(planes):
+        row = jnp.sum(jnp.where(ids_ref[...] == e, route_ref[...], 0.0), axis=0, keepdims=True)
+        column = lane_to_column(row, rows)
+        high = column.astype(jnp.bfloat16).astype(jnp.float32)
+        routes = jnp.where(lanes == e, high, routes)
+        routes = jnp.where(lanes == planes + e, column - high, routes)
+    tok[me, :, width:] = routes.astype(jnp.bfloat16)
     for h in range(HALVES):
         values = tokens_ref[span(h), :].astype(jnp.float32)
         center = values - jnp.mean(values, axis=-1, keepdims=True)
         spread = jnp.mean(center * center, axis=-1, keepdims=True)
-        tok[me, span(h), :] = (center * lax.rsqrt(spread + EPSILON) * gain_ref[...]).astype(
+        tok[me, span(h), :width] = (center * lax.rsqrt(spread + EPSILON) * gain_ref[...]).astype(
             jnp.bfloat16
         )
-    for e in range(planes):
-        column = jnp.sum(jnp.where(ids_ref[...] == e, route_ref[...], 0.0), axis=1, keepdims=True)
-        wsend[e] = jnp.broadcast_to(column_to_lane(column, rows), (8, rows))
-    pl.semaphore_wait(barrier, devices - 1)
-
-    has_up, has_down = z < planes - 1, z > 0
-    for h in range(HALVES):
+        if h == 0:
+            pl.semaphore_wait(
+                barrier, 2 + has_up.astype(jnp.int32) + has_down.astype(jnp.int32)
+            )
         move(2, me, h, ypeer).start()
         pl.when(has_up)(lambda: move(0, me, h, me + 4).start())
         pl.when(has_down)(lambda: move(1, me, h, me - 4).start())
         move(3, me, h, cpeer).start()
-
-    def share(step):
-        there = (me + step) % devices
-        return remote(wsend.at[there // SPLIT], wbuf.at[me], ssend.at[there], srecv.at[me], there)
-
-    def shared(step):
-        there = (me + step) % devices
-        return remote(wsend.at[z], wbuf.at[there], ssend.at[there], srecv.at[there], there)
-
-    for step in range(1, devices):
-        share(step).start()
-    wbuf[me] = wsend[z]
     for load in weight_loads:
         load.wait()
-    for step in range(1, devices):
-        shared(step).wait_recv()
 
     def onward(zp):
         return jnp.where(zp < z, z + 1, z - 1)
@@ -197,7 +191,8 @@
 
     def compute(zp, yp):
         first = index(zp, yp, 0)
-        x = tok[pl.ds(first, 2)].reshape(2 * rows, width)
+        x = tok[pl.ds(first, 2), :, :width].reshape(2 * rows, width)
+        routes = tok[pl.ds(first, 2), :, width:].reshape(2 * rows, LANES).astype(jnp.float32)
         gate_cut = jnp.minimum(
             jnp.dot(x, gate[...], preferred_element_type=jnp.float32), clamp_limit
         )
@@ -207,9 +202,8 @@
         active = ((up_cut + 1.0) * (gate_cut * jax.nn.sigmoid(gate_cut * sigmoid_slope))).astype(
             jnp.bfloat16
         )
-        scale = jnp.concatenate(
-            [lane_to_column(wbuf[first + lane, 0:1, :], rows) for lane in range(2)], axis=0
-        )
+        mine = jnp.logical_or(lanes == z, lanes == planes + z)
+        scale = jnp.sum(jnp.where(mine, routes, 0.0), axis=1, keepdims=True)
         tile = min(512, width)
         for start in range(0, width, tile):
             value = jnp.dot(
@@ -220,11 +214,30 @@
             )
 
     def to_core(zp, yp):
-        group = zp * 2 + yp
-        return remote(
-            part.at[index(zp, yp, 1 - c)], cbuf.at[group],
-            rsend_c.at[group], rrecv_c.at[group], cpeer,
-        )
+        pair = zp * 2 + yp
+        return remote(
+            part.at[index(zp, yp, 1 - c)], cbuf.at[pair],
+            rsend_c.at[pair], rrecv_c.at[pair], cpeer,
+        )
+
+    def beside(plane):
+        return jnp.abs(plane - z) == 1
+
+    def pass_up():
+        return move(4, index(z, 1 - y, c), 1, me + 4)
+
+    def pass_down():
+        return move(5, index(z, 1 - y, c), 1, me - 4)
+
+    def take(i, h):
+        move(3, i, h, cpeer).wait_recv()
+        move(3, i, h, cpeer).start()
+
+    def group(zp, yp):
+        for h in range(HALVES):
+            move(3, index(zp, yp, 1 - c), h, cpeer).wait_recv()
+        compute(zp, yp)
+        to_core(zp, yp).start()
 
     def gather_step(k, _):
         zk = near_plane(z, jnp.minimum(k, planes - 1), planes)
@@ -237,27 +250,34 @@
             for h in range(HALVES):
                 move(2, i, h, ypeer).wait_recv()
                 pl.when(exists(nz))(lambda: move(0, i, h, index(nz, y, c)).start())
-                move(2, i, h, ypeer).start()
+                if h == 0:
+                    move(2, i, h, ypeer).start()
+                else:
+                    pl.when(jnp.logical_not(beside(zk)))(lambda: move(2, i, h, ypeer).start())
                 move(3, i, h, cpeer).start()
 
+        @pl.when(k == planes - 1)
+        def _():
+            inner = jnp.logical_and(has_up, has_down)
+            pl.when(inner)(lambda: pass_up().start())
+            pl.when(inner)(lambda: pass_down().start())
+
         @pl.when(k > 0)
         def _():
             i = index(zb, 1 - y, c)
-            for h in range(HALVES):
-                move(3, i, h, cpeer).wait_recv()
-                move(3, i, h, cpeer).start()
+            take(i, 0)
+            pl.when(jnp.logical_not(beside(zb)))(lambda: take(i, 1))
+
+        @pl.when(k == 1)
+        def _():
+            pl.when(jnp.logical_not(has_down))(lambda: pass_up().start())
+            pl.when(jnp.logical_not(has_up))(lambda: pass_down().start())
 
         def group_step(j, _):
             zp = jnp.where(j == 0, zk, zb)
             yp = jnp.where(j == 0, y, 1 - y)
-
-            @pl.when(jnp.where(j == 0, planes - k, k) > 0)
-            def _():
-                for h in range(HALVES):
-                    move(3, index(zp, yp, 1 - c), h, cpeer).wait_recv()
-                compute(zp, yp)
-                to_core(zp, yp).start()
-
+            ready = jnp.where(beside(zb), 0, k)
+            pl.when(jnp.where(j == 0, planes - k, ready) > 0)(lambda: group(zp, yp))
             return 0
 
         lax.fori_loop(0, 2, group_step, 0)
@@ -279,8 +299,14 @@
 
     def spread_step(t, _):
         zp = near_plane(z, planes - 1 - t, planes)
+        i = index(zp, 1 - y, c)
+
+        @pl.when(beside(zp))
+        def _():
+            take(i, 1)
+            group(zp, 1 - y)
+
         to_core(zp, 1 - y).wait_recv()
-        i = index(zp, 1 - y, c)
         for h in range(HALVES):
             part[i, span(h), :] = (
                 part[i, span(h), :].astype(jnp.float32)
@@ -335,13 +361,14 @@
         pl.when(has_up)(lambda: add_landed(planes, h))
         out_ref[span(h), :] = acc[...].astype(jnp.bfloat16)
 
-    for step in range(1, devices):
-        share(step).wait_send()
     for h in range(HALVES):
         move(2, me, h, ypeer).wait_send()
         pl.when(has_up)(lambda: move(0, me, h, me + 4).wait_send())
         pl.when(has_down)(lambda: move(1, me, h, me - 4).wait_send())
         move(3, me, h, cpeer).wait_send()
+
+    pl.when(has_up)(lambda: pass_up().wait_send())
+    pl.when(has_down)(lambda: pass_down().wait_send())
 
     def drain_step(k, _):
         zp = near_plane(z, k, planes)
@@ -357,7 +384,12 @@
             nz = onward(zp)
             for h in range(HALVES):
                 pl.when(exists(nz))(lambda: move(0, i, h, index(nz, y, c)).wait_send())
-                move(2, i, h, ypeer).wait_send()
+                if h == 0:
+                    move(2, i, h, ypeer).wait_send()
+                else:
+                    pl.when(jnp.logical_not(beside(zp)))(
+                        lambda: move(2, i, h, ypeer).wait_send()
+                    )
                 move(3, i, h, cpeer).wait_send()
                 hop(zp, h).wait_send()
 
@@ -380,19 +412,17 @@
         in_specs=[pl.BlockSpec(memory_space=vmem)] * 4 + [pl.BlockSpec(memory_space=pl.ANY)] * 3,
         out_specs=pl.BlockSpec(memory_space=vmem),
         scratch_shapes=[
-            vmem((devices, rows, width), block),
+            vmem((devices, rows, width + LANES), block),
             vmem((devices, rows, width), block),
             vmem((2 * planes, rows, width), block),
             vmem((planes, rows, width), block),
             vmem((planes + 1, rows, width), block),
             vmem((half, width), jnp.float32),
-            vmem((planes, 8, rows), jnp.float32),
-            vmem((devices, 8, rows), jnp.float32),
             vmem((width, hidden), block),
             vmem((width, hidden), block),
             vmem((hidden, width), block),
             dma((3,)),
-            dma((4, devices, HALVES)),
+            dma((6, devices, HALVES)),
             dma((devices, HALVES)),
             dma((2 * planes,)),
             dma((2 * planes,)),
@@ -400,15 +430,13 @@
             dma((planes, HALVES)),
             dma((planes, HALVES)),
             dma((planes + 1, HALVES)),
-            dma((devices,)),
-            dma((devices,)),
         ],
         compiler_params=pltpu.CompilerParams(
             collective_id=0, has_side_effects=True, vmem_limit_bytes=60 * 1024 * 1024
         ),
         name="dense_experts",
     )(
-        tokens, norm_gain.reshape(1, width), expert_ids, route_weight,
+        tokens, norm_gain.reshape(1, width), expert_ids.T, route_weight.T,
         gate_weight, up_weight, down_weight,
     )
 

time: 120 us -> 109 us (0.908)
  Pallas kernels: 115 us -> 107 us
  local copies, waits for them, and re-layouts: 4.7 us -> 1.88 us
    pallas_call x1, Pallas kernels: 115 us -> 107 us  [dense_body(): pl.pallas_call(functools.partial(dense_kernel, devices), out_shape=jax.Sh...]
    unnamed x3 -> x1, local copies, waits for them, and re-layouts: 4.7 us -> 1.88 us
where the time goes in v2:
time: 109 us
  Pallas kernels  107 us (98%)
  local copies, waits for them, and re-layouts  1.88 us (2%)
    pallas_call x1, Pallas kernels, dense_body(): pl.pallas_call(functools.partial(dense_kernel, devices), out_shape=jax.Sh...  107 us

profile of v2, /device:TPU:0, one launch (start us, length us, event | category | flops | bytes accessed | tf_op | source)
XLA Modules:
  0.0 109.0 jit_solution(979786790463670707)
XLA Ops:
  0.0 107.1 %dense_experts.1 = bf16[128,2048]{1,0:T(8,128)(2,1)} custom-call(bf16[128,2048]{1,0:T(8,128)(2,1)} %tokens_ref.1, f32[1,2048]{1,0:T(1,128)} %bitcast.3, s32[2,128]{1,0:T(2,128)} %bitcast.4, f32[2,128]{1,0:T(2,128)} %bitcast.5, bf16[1,2048,512]{2,1,0:T(8,128)(2,1)} %gate_hbm.1, bf16[1,2048,512]{2,1,0:T(8,128)(2,1)} %up_hbm.1, bf16[1,512,2048]{2,1,0:T(8,128)(2,1)} %down_hbm.1), custom_call_target="tpu_custom_call" | custom-call | tf_op jit(solution)/shard_map/dense_experts/pallas_call | solution.py:409
  107.1 1.9 %copy.9 = bf16[128,2048]{1,0:T(8,128)(2,1)} copy(bf16[128,2048]{1,0:T(8,128)(2,1)} %dense_experts.1) | data formatting | bytes 1048576

commit v3 on v2

--- a/solution.py
+++ b/solution.py
@@ -239,9 +239,28 @@
         compute(zp, yp)
         to_core(zp, yp).start()
 
+    def to_y(zp, h):
+        return remote(
+            part.at[index(zp, 1 - y, c), span(h)], ybuf.at[zp, span(h)],
+            rsend_y.at[zp, h], rrecv_y.at[zp, h], ypeer,
+        )
+
+    def spread_half(zp, h):
+        i = index(zp, 1 - y, c)
+        part[i, span(h), :] = (
+            part[i, span(h), :].astype(jnp.float32)
+            + cbuf[zp * 2 + 1 - y, span(h), :].astype(jnp.float32)
+        ).astype(jnp.bfloat16)
+        to_y(zp, h).start()
+
     def gather_step(k, _):
         zk = near_plane(z, jnp.minimum(k, planes - 1), planes)
         zb = near_plane(z, jnp.maximum(k - 1, 0), planes)
+
+        @pl.when(k == planes)
+        def _():
+            to_core(z, 1 - y).wait_recv()
+            spread_half(z, 0)
 
         @pl.when(jnp.logical_and(k > 0, k < planes))
         def _():
@@ -285,12 +304,6 @@
 
     lax.fori_loop(0, planes + 1, gather_step, 0)
 
-    def to_y(zp, h):
-        return remote(
-            part.at[index(zp, 1 - y, c), span(h)], ybuf.at[zp, span(h)],
-            rsend_y.at[zp, h], rrecv_y.at[zp, h], ypeer,
-        )
-
     def from_y(zp, h):
         return remote(
             part.at[index(zp, y, c), span(h)], ybuf.at[zp, span(h)],
@@ -306,13 +319,12 @@
             take(i, 1)
             group(zp, 1 - y)
 
-        to_core(zp, 1 - y).wait_recv()
-        for h in range(HALVES):
-            part[i, span(h), :] = (
-                part[i, span(h), :].astype(jnp.float32)
-                + cbuf[zp * 2 + 1 - y, span(h), :].astype(jnp.float32)
-            ).astype(jnp.bfloat16)
-            to_y(zp, h).start()
+        @pl.when(zp != z)
+        def _():
+            to_core(zp, 1 - y).wait_recv()
+            spread_half(zp, 0)
+
+        spread_half(zp, 1)
         return 0
 
     lax.fori_loop(0, planes, spread_step, 0)

time: 109 us -> 104 us (0.954)
  Pallas kernels: 107 us -> 102 us
    pallas_call x1, Pallas kernels: 107 us -> 102 us  [dense_body(): pl.pallas_call(functools.partial(dense_kernel, devices), out_shape=jax.Sh...]
where the time goes in v3:
time: 104 us
  Pallas kernels  102 us (98%)
  local copies, waits for them, and re-layouts  1.88 us (2%)
    pallas_call x1, Pallas kernels, dense_body(): pl.pallas_call(functools.partial(dense_kernel, devices), out_shape=jax.Sh...  102 us

profile of v3, /device:TPU:0, one launch (start us, length us, event | category | flops | bytes accessed | tf_op | source)
XLA Modules:
  0.0 103.8 jit_solution(14411358850814133020)
XLA Ops:
  0.0 101.9 %dense_experts.1 = bf16[128,2048]{1,0:T(8,128)(2,1)} custom-call(bf16[128,2048]{1,0:T(8,128)(2,1)} %tokens_ref.1, f32[1,2048]{1,0:T(1,128)} %bitcast.3, s32[2,128]{1,0:T(2,128)} %bitcast.4, f32[2,128]{1,0:T(2,128)} %bitcast.5, bf16[1,2048,512]{2,1,0:T(8,128)(2,1)} %gate_hbm.1, bf16[1,2048,512]{2,1,0:T(8,128)(2,1)} %up_hbm.1, bf16[1,512,2048]{2,1,0:T(8,128)(2,1)} %down_hbm.1), custom_call_target="tpu_custom_call" | custom-call | tf_op jit(solution)/shard_map/dense_experts/pallas_call | solution.py:421
  101.9 1.9 %copy.9 = bf16[128,2048]{1,0:T(8,128)(2,1)} copy(bf16[128,2048]{1,0:T(8,128)(2,1)} %dense_experts.1) | data formatting | bytes 1048576
